TPU v7x, 128 devices: a whole 4x4x4 slice. The times are simulated.
128 devices in a mesh: sp: 16 (over z, y), tp: 8 (over x, core).
Axes of the slice: x: 4, y: 4, z: 4, core: 2. Of those that a mesh axis runs over, the one named last changes fastest.
Arguments:
- tokens: bfloat16 [12288, 2048], P(('sp', 'tp')), may hold values from -6 to 6
- norm_gain: float32 [2048], replicated, may hold values from 0.1 to 1.9
- w_query: bfloat16 [2048, 1024], P('sp', 'tp'), may hold values from -0.125 to 0.125
- w_forget: bfloat16 [2048, 1024], P('sp', 'tp'), may hold values from -0.125 to 0.125
- w_input: bfloat16 [2048, 1024], P('sp', 'tp'), may hold values from -0.125 to 0.125
- w_outgate: bfloat16 [2048, 1024], P('sp', 'tp'), may hold values from -0.125 to 0.125
- w_conv_value: bfloat16 [2048, 1024], P('sp', 'tp'), may hold values from -0.125 to 0.125
- w_conv_gate: bfloat16 [2048, 1024], P('sp', 'tp'), may hold values from -0.125 to 0.125
- w_gate_rec: bfloat16 [2048, 2048], P('sp', 'tp'), may hold values from -0.125 to 0.125
- w_gate_conv: bfloat16 [2048, 2048], P('sp', 'tp'), may hold values from -0.125 to 0.125
- lower_bound: float32 [1024], P('tp'), may hold values from 0.92 to 0.9999593, as said below
- decay_shift: float32 [12288, 1024], P('sp', 'tp'), may hold values from -0.7 to 0, as said below
- state_init: float32 [8, 128, 128], P('tp'), may hold values from -0.125 to 0.125
- head_gain: float32 [1024], P('tp'), may hold values from 0.1 to 1.9
- conv_kernel: float32 [31, 1024], P(None, 'tp'), may hold values from -7.5 to 7.5
- channel_gain: float32 [1024], P('tp'), may hold values from 0.1 to 1.9
- channel_bias: float32 [1024], P('tp'), may hold values from -3 to 3
- w_out_rec: bfloat16 [1024, 2048], P('tp', 'sp'), may hold values from -0.1875 to 0.1875
- w_out_conv: bfloat16 [1024, 2048], P('tp', 'sp'), may hold values from -0.1875 to 0.1875
Outputs:
- mixed_out: bfloat16 [12288, 2048], P('sp', 'tp')
Inputs may be any that keep to these rules, and one draw needn't show every extreme that they name: `lower_bound`: every entry is below one. `decay_shift`: no entry is positive.
All inputs are finite; a program needn't handle non-finite values.
Results may differ from a plain program's by a relative error of at most 0.017.
Values may be sent and summed in bfloat16 or wider, within the bound.
A program may use at most 64 MiB of HBM per device.

v0:
```python
import jax
import jax.numpy as jnp
from jax import lax
from jax.sharding import PartitionSpec as P

HEAD = 128
CONV = 1024
KW = 31
BLOCK = 64
EPSILON = 1e-06


def in_one_piece(arrays, axis, dim, along):
    ends, at = ([], 0)
    for a in arrays[:-1]:
        at += a.shape[along]
        ends.append(at)
    both = jnp.concatenate(arrays, axis=along)
    return tuple(jnp.split(lax.all_gather(both, axis, axis=dim, tiled=True), ends, axis=along))


def sent_to_all(array, axis):
    size = lax.axis_size(axis)
    return lax.all_to_all(
        jnp.broadcast_to(array[None], (size, *array.shape)), axis, 0, 0, tiled=True
    )


def all_in_one(array, axis):
    leaves = jax.tree.leaves(array)
    sequence = sorted(range(len(leaves)), key=lambda k: -leaves[k].size)
    width = (1, *leaves[sequence[0]].shape)[-1]
    lines = [
        jnp.pad(leaves[k].reshape(-1), (0, -leaves[k].size % width)).reshape(-1, width)
        for k in sequence
    ]
    both, at, found = (sent_to_all(jnp.concatenate(lines), axis), 0, {})
    for k, line in zip(sequence, lines):
        section = both[:, at : at + len(line)].reshape(len(both), -1)
        found[k] = section[:, : leaves[k].size].reshape(-1, *leaves[k].shape)
        at += len(line)
    numbers = iter(range(len(leaves)))
    return jax.tree.map(lambda _: found[next(numbers)], array)


def joined_by_halves(pieces, combine):
    while len(jax.tree.leaves(pieces)[0]) > 1:
        pieces = jax.vmap(combine)(
            *(jax.tree.map(lambda part: part[side::2], pieces) for side in (0, 1))
        )
    return jax.tree.map(lambda part: part[0], pieces)


def entering(array, axis, combine, identity):
    size, position = (lax.axis_size(axis), lax.axis_index(axis))
    passed = jnp.arange(size) < position

    def kept(part, zero, own):
        part = jnp.where(
            passed.reshape(-1, *(1 for _ in own.shape)),
            part.astype(own.dtype),
            jnp.asarray(zero, own.dtype),
        )
        return part

    pieces = all_in_one(
        jax.tree.map(lambda part, kind: part.astype(kind), array, (jnp.bfloat16, jnp.bfloat16)),
        axis,
    )
    return joined_by_halves(jax.tree.map(kept, pieces, identity, array), combine)


def passed_along(block, axis, distance):
    devices = range(lax.axis_size(axis))
    route = [(i - distance, i) for i in devices if i - distance in devices]
    return lax.ppermute(block, axis, route)


def of_everyone(array, axis):
    everything = sent_to_all(array, axis)
    return jnp.sum(everything, axis=0)


def normalize_rows(values, gain_vector):
    widened = values.astype(jnp.float32)
    scale = lax.rsqrt(jnp.mean(widened * widened, axis=-1, keepdims=True) + EPSILON)
    return (widened * scale * gain_vector).astype(jnp.bfloat16)


def block_step(state, inputs):
    query, input_gate, values, log_decay = inputs
    length = query.shape[1]
    causal_masked = (jnp.arange(length)[:, None] >= jnp.arange(length)[None, :])[None, :, :, None]
    cumulative = jnp.cumsum(log_decay, axis=1)
    spread = cumulative[:, :, None, :] - cumulative[:, None, :, :]
    weight = jnp.where(causal_masked, jnp.exp(jnp.where(causal_masked, spread, 0.0)), 0.0)
    scores = jnp.einsum("htd,hsd,htsd->hts", query, input_gate, weight)
    output = jnp.einsum("hts,hsv->htv", scores, values)
    output = output + jnp.einsum("htd,hdv->htv", query * jnp.exp(cumulative), state)
    final = cumulative[:, -1:, :]
    carried = jnp.exp(final[:, 0, :])[:, :, None] * state
    carried = carried + jnp.einsum("hsd,hsv->hdv", input_gate * jnp.exp(final - cumulative), values)
    return (carried, output)


def compose(preceding_segment, later):
    return (preceding_segment[0] * later[0], later[0][..., None] * preceding_segment[1] + later[1])


def local(
    tokens,
    norm_gain,
    w_query,
    w_forget,
    w_input,
    w_outgate,
    w_conv_value,
    w_conv_gate,
    w_gate_rec,
    w_gate_conv,
    lower_bound,
    decay_shift,
    state_init,
    head_gain,
    conv_kernel,
    channel_gain,
    channel_bias,
    w_out_rec,
    w_out_conv,
):
    tp_count = lax.axis_size("tp")
    normed = normalize_rows(lax.all_gather(tokens, "tp", axis=0, tiled=True), norm_gain)
    row_count = normed.shape[0]
    weights = (
        w_query,
        w_forget,
        w_input,
        w_outgate,
        w_conv_value,
        w_conv_gate,
        w_gate_rec,
        w_gate_conv,
    )
    portions = in_one_piece(
        (
            weights[0],
            weights[1],
            weights[2],
            weights[3],
            weights[4],
            weights[5],
            weights[6],
            weights[7],
        ),
        "sp",
        0,
        1,
    )
    sums = tuple(
        (jnp.dot(normed, portion, preferred_element_type=jnp.float32) for portion in portions)
    )
    (
        query_raw,
        forget_raw,
        input_raw,
        outgate_raw,
        value_raw,
        gate_raw,
        gate_rec_raw,
        gate_conv_raw,
    ) = tuple((overall_aggregate.astype(jnp.bfloat16) for overall_aggregate in sums))
    local_heads = w_query.shape[1] // HEAD
    block_count = row_count // BLOCK
    query = jax.nn.silu(query_raw.astype(jnp.float32))
    input_gate = (1.0 - lower_bound) * jax.nn.sigmoid(-forget_raw.astype(jnp.float32))
    log_decay = jnp.log1p(-input_gate) + decay_shift
    values = input_raw.astype(jnp.float32)

    def to_blocks(array):
        return array.reshape(block_count, BLOCK, local_heads, HEAD).transpose(0, 2, 1, 3)

    zero_state = jnp.zeros((local_heads, HEAD, HEAD), jnp.float32)
    local_state, blocks_out = lax.scan(
        block_step,
        zero_state,
        (to_blocks(query), to_blocks(input_gate), to_blocks(values), to_blocks(log_decay)),
    )
    local_out = blocks_out.transpose(0, 2, 1, 3).reshape(row_count, local_heads, HEAD)
    running = jnp.cumsum(log_decay, axis=0)
    cumulated_forgetting = jnp.exp(running[-1]).reshape(local_heads, HEAD)
    ones_decay = jnp.ones_like(cumulated_forgetting)
    prefix_decay, prefix_state = entering(
        (cumulated_forgetting, local_state), "sp", compose, (ones_decay, zero_state)
    )
    incoming_state = prefix_decay[:, :, None] * state_init + prefix_state
    decayed_query = (query * jnp.exp(running)).reshape(row_count, local_heads, HEAD)
    head_out = local_out + jnp.einsum("thd,hdv->thv", decayed_query, incoming_state)
    head_out = head_out * lax.rsqrt(jnp.mean(head_out * head_out, axis=-1, keepdims=True) + EPSILON)
    head_out = head_out * head_gain.reshape(local_heads, HEAD)
    mixed_rec = (
        head_out.reshape(row_count, local_heads * HEAD)
        * jax.nn.silu(outgate_raw.astype(jnp.float32))
    ).astype(jnp.bfloat16)
    gated = (value_raw.astype(jnp.float32) * jax.nn.sigmoid(gate_raw.astype(jnp.float32))).astype(
        jnp.bfloat16
    )
    rim_width = KW - 1
    previous = passed_along(gated[row_count - rim_width :], "sp", 1)
    extended = jnp.concatenate([previous, gated], axis=0).astype(jnp.float32)
    conv_out = jnp.zeros((row_count, gated.shape[1]), jnp.float32)
    for tap_index in range(KW):
        conv_out = conv_out + conv_kernel[tap_index] * extended[tap_index : tap_index + row_count]
    squares = of_everyone(jnp.sum(conv_out * conv_out, axis=1), "tp")
    scale = lax.rsqrt(squares / CONV + EPSILON)[:, None]
    mixed_conv = jax.nn.silu(conv_out * scale * channel_gain + channel_bias).astype(jnp.bfloat16)
    rec_columns, conv_columns = in_one_piece((w_out_rec, w_out_conv), "sp", 1, 0)
    rec_width = mixed_rec.shape[1]
    rec_whole, conv_whole = in_one_piece((rec_columns, conv_columns), "tp", 0, 1)
    both = jnp.concatenate([mixed_rec, mixed_conv], axis=1).reshape(
        tp_count, row_count // tp_count, -1
    )
    arrived = lax.all_to_all(both, "tp", split_axis=0, concat_axis=2, tiled=True)
    item_count = arrived.shape[1]
    grouped = arrived.reshape(item_count, tp_count, -1)
    rec_part = grouped[:, :, :rec_width].reshape(item_count, -1)
    conv_part = grouped[:, :, rec_width:].reshape(item_count, -1)
    first = jnp.dot(rec_part, rec_whole, preferred_element_type=jnp.float32).astype(jnp.bfloat16)
    second = jnp.dot(conv_part, conv_whole, preferred_element_type=jnp.float32).astype(jnp.bfloat16)
    projected = jnp.stack([first, second], axis=1)[None]
    returned = lax.all_to_all(projected[0], "tp", split_axis=2, concat_axis=0, tiled=True)
    y_rec = returned[:, 0]
    y_conv = returned[:, 1]
    merged = jax.nn.sigmoid(gate_rec_raw.astype(jnp.float32)) * y_rec.astype(jnp.float32)
    merged = merged + jax.nn.sigmoid(gate_conv_raw.astype(jnp.float32)) * y_conv.astype(jnp.float32)
    return merged.astype(jnp.bfloat16)


def solution(mesh):
    in_specs = (
        P(("sp", "tp"), None),
        P(),
        P("sp", "tp"),
        P("sp", "tp"),
        P("sp", "tp"),
        P("sp", "tp"),
        P("sp", "tp"),
        P("sp", "tp"),
        P("sp", "tp"),
        P("sp", "tp"),
        P("tp"),
        P("sp", "tp"),
        P("tp", None, None),
        P("tp"),
        P(None, "tp"),
        P("tp"),
        P("tp"),
        P("tp", "sp"),
        P("tp", "sp"),
    )
    out_specs = P("sp", "tp")
    return jax.shard_map(local, mesh=mesh, in_specs=in_specs, out_specs=out_specs, check_vma=False)
```

profile of v0, /device:TPU:1, one launch (start us, length us, event | category | flops | bytes accessed | tf_op | source)
XLA Modules:
  0.0 333.0 jit_solution(5961914956780123622)
XLA Ops:
  6.5 1.4 pad_maximum_fusion.3
  16.6 1.6 slice_bitcast_fusion.35
  18.1 1.7 slice_bitcast_fusion.36
  19.8 34.6 %all-gather.9.cloned.1.call-done = bf16[256,2048]{1,0:T(8,128)(2,1)} async-done(((bf16[256,128]{1,0:T(8,128)(2,1)}), bf16[256,2048]{1,0:T(8,128)(2,1)}) %all-gather.9.cloned.1.call-update) | async-done | bytes 1048592 | tf_op jit(solution)/shard_map/all_gather | solution.py:19
  54.3 1.3 fusion.138
  55.7 1.1 pad_maximum_fusion
  56.8 28.2 %all-gather.5.cloned.1.call-done = bf16[768,2048]{1,0:T(8,128)(2,1)} async-done(((bf16[96,2048]{1,0:T(8,128)(2,1)}), bf16[768,2048]{1,0:T(8,128)(2,1)}) %all-gather.5.cloned.1.call-update) | async-done | bytes 3145744 | tf_op jit(solution)/shard_map/all_gather | solution.py:132
  85.0 2.7 fusion.28
  88.6 54.3 %all-gather.7.cloned.1.call-done = bf16[2048,1280]{1,0:T(8,128)(2,1)} async-done(((bf16[128,1280]{1,0:T(8,128)(2,1)}), bf16[2048,1280]{1,0:T(8,128)(2,1)}) %all-gather.7.cloned.1.call-update) | async-done | bytes 5242896 | tf_op jit(solution)/shard_map/all_gather | solution.py:19
  142.9 2.8 divide_multiply_fusion
  145.7 2.1 convolution_convert_fusion.6
  147.7 2.9 log-plus-one_add_fusion
  150.7 80.2 %while.13 = (s32[]{:T(128)}, f32[1,128,128]{2,1,0:T(8,128)S(1)}, f32[12,1,64,128]{3,2,1,0:T(8,128)}, f32[12,1,64,128]{3,2,1,0:T(8,128)}, f32[12,1,64,128]{3,2,1,...) while((s32[]{:T(128)}, f32[1,128,128]{2,1,0:T(8,128)S(1)}, ...), condition=%wide.region_3.4_spmd.clone, body=%wide.region_1.3_spmd.clone.sunk | while | flops 9003011 | bytes 5051520 | solution.py:183
  153.0 1.7 fusion.167
  154.9 1.5 fusion.169
  156.4 1.0 fusion.166
  159.7 1.7 fusion.167
  161.5 1.5 fusion.169
  163.1 1.0 fusion.166
  166.3 1.7 fusion.167
  168.2 1.5 fusion.169
  169.8 1.0 fusion.166
  173.0 1.7 fusion.167
  174.9 1.5 fusion.169
  176.4 1.0 fusion.166
  179.7 1.7 fusion.167
  181.6 1.5 fusion.169
  183.1 1.0 fusion.166
  186.4 1.7 fusion.167
  188.3 1.5 fusion.169
  193.1 1.7 fusion.167
  195.0 1.5 fusion.169
  199.8 1.7 fusion.167
  201.6 1.5 fusion.169
  206.4 1.7 fusion.167
  208.3 1.5 fusion.169
  213.1 1.7 fusion.167
  215.0 1.5 fusion.169
  219.8 1.7 fusion.167
  221.7 1.5 fusion.169
  226.5 1.7 fusion.167
  228.4 1.5 fusion.169
  230.9 1.2 fusion.85
  232.9 1.1 broadcast_add_fusion
  234.1 2.2 fusion.69
  236.5 2.0 fusion.68
  238.6 3.1 collective-permute-start
  243.2 1.5 multiply_reduce_fusion
  245.3 5.5 %all-to-all-start.1 = ((f32[8,1,768]{2,1,0:T(1,128)}), f32[8,1,768]{2,1,0:T(1,128)}, u32[]{:S(2)}, u32[]{:S(2)}) async-start(f32[8,1,768]{2,1,0:T(1,128)} %broadcast_in_dim.89), calls=%async_computation.1 | async-start | bytes 49152 | tf_op jit(solution)/shard_map/all_to_all | solution.py:24
  250.8 1.4 pad_maximum_fusion.4
  252.2 3.4 %all-to-all-done.1 = f32[8,1,768]{2,1,0:T(1,128)} async-done(((f32[8,1,768]{2,1,0:T(1,128)}), f32[8,1,768]{2,1,0:T(1,128)}, u32[]{:S(2)}, u32[]{:S(2)}) %all-to-all-start.1) | async-done | bytes 24608 | tf_op jit(solution)/shard_map/all_to_all | solution.py:24
  255.6 1.6 broadcast_in_dim.85
  257.3 7.0 %all-to-all-start = ((bf16[16,129,128]{2,1,0:T(8,128)(2,1)}), bf16[16,129,128]{2,1,0:T(8,128)(2,1)}, u32[]{:S(2)}, u32[]{:S(2)}) async-start(bf16[16,129,128]{2,1,0:T(8,128)(2,1)} %broadcast_in_dim.85), calls=%async_computation | async-start | bytes 1114112 | tf_op jit(solution)/shard_map/all_to_all | solution.py:24
  265.1 1.5 multiply_convert_fusion
  266.6 8.4 %all-to-all-done = bf16[16,129,128]{2,1,0:T(8,128)(2,1)} async-done(((bf16[16,129,128]{2,1,0:T(8,128)(2,1)}), bf16[16,129,128]{2,1,0:T(8,128)(2,1)}, u32[]{:S(2)}, u32[]{:S(2)}) %all-to-all-start) | async-done | bytes 528416 | tf_op jit(solution)/shard_map/all_to_all | solution.py:24
  276.1 1.2 select_bitcast_fusion
  278.2 2.1 fusion.117
  280.3 12.6 %all_to_all.44 = bf16[8,96,256]{2,1,0:T(8,128)(2,1)S(1)} all-to-all(bf16[8,96,256]{2,1,0:T(8,128)(2,1)S(1)} %bitcast.263), channel_id=1, replica_groups=mesh['sp'=16,'tp'=8] {'tp'}, dimensions={0} | all-to-all | bytes 786432 | tf_op jit(solution)/shard_map/all_to_all | solution.py:222
  293.0 3.0 fusion.44
  296.0 3.0 fusion.41
  299.8 18.2 %all_to_all.45 = bf16[96,2,2048]{0,1,2:T(2,128)(2,1)S(1)} all-to-all(bf16[96,2,2048]{0,1,2:T(2,128)(2,1)S(1)} %copy.78), channel_id=1, replica_groups=mesh['sp'=16,'tp'=8] {'tp'}, dimensions={2} | all-to-all | bytes 1572864 | tf_op jit(solution)/shard_map/all_to_all | solution.py:230
  318.1 1.9 copy.79
  320.0 3.4 %fusion.60 = f32[768,256]{1,0:T(8,128)S(1)} fusion(bf16[768,2048]{1,0:T(8,128)(2,1)} %copy-done.1, bf16[2048,1280]{1,0:T(8,128)(2,1)} %all-gather.7.cloned.1.call-done, bf16[768,2,256]{2,0,1:T(8,128)(2,1)} %bitcast.268), kind=kOutput, calls=%fused_computation.65 | convolution fusion | flops 806682624 | bytes 5373952 | tf_op jit(solution)/shard_map/dot_general | solution.py:160
  323.5 3.0 fusion.54
  (235 shorter events, 52.1 us)
Async XLA Ops:
  6.5 47.8 %all-gather.9.cloned.1.call-start = ((), (), s32[]{:S(2)}) async-start(), calls=%async_computation.6 | async-start | bytes 1114112 | tf_op jit(solution)/shard_map/all_gather | solution.py:19
  8.0 77.0 %all-gather.5.cloned.1.call-start = ((), (), s32[]{:S(2)}) async-start(), calls=%async_computation.4 | async-start | bytes 3538944 | tf_op jit(solution)/shard_map/all_gather | solution.py:132
  8.7 134.1 %all-gather.7.cloned.1.call-start = ((), (), s32[]{:S(2)}) async-start(), calls=%async_computation.5 | async-start | bytes 5570560 | tf_op jit(solution)/shard_map/all_gather | solution.py:19
  15.1 0.7 copy-start.9
  15.8 277.2 %all-gather.11.cloned.1.call-start = ((), (), s32[]{:S(2)}) async-start(), calls=%async_computation.7 | async-start | bytes 9437184 | tf_op jit(solution)/shard_map/all_gather | solution.py:19
  55.7 32.0 %copy-start.12 = (f32[2048]{0:T(1024)S(1)}, f32[2048]{0:T(1024)}, u32[]{:S(2)}) copy-start(f32[2048]{0:T(1024)} %param.22) | copy-start | bytes 24580
  85.0 2.8 copy-start
  88.6 189.6 %copy-start.1 = (bf16[768,2048]{1,0:T(8,128)(2,1)}, bf16[768,2048]{1,0:T(8,128)(2,1)S(1)}, u32[]{:S(2)}) copy-start(bf16[768,2048]{1,0:T(8,128)(2,1)S(1)} %fusion.30) | copy-start | bytes 9437188
  145.7 2.1 copy-start.40
  232.1 0.8 copy-start.3
  234.1 8.2 %copy-start.4 = (f32[128,6,128]{0,2,1:T(8,128)}, f32[128,6,128]{0,2,1:T(8,128)S(1)}, u32[]{:S(2)}) copy-start(f32[128,6,128]{0,2,1:T(8,128)S(1)} %copy.72) | copy-start | bytes 1179652
  236.3 6.6 %copy-start.13 = (f32[128]{0:T(128)S(1)}, f32[128]{0:T(128)}, u32[]{:S(2)}) copy-start(f32[128]{0:T(128)} %get-tuple-element.149) | copy-start | bytes 1540
  236.3 6.6 %copy-start.14 = (f32[128]{0:T(128)S(1)}, f32[128]{0:T(128)}, u32[]{:S(2)}) copy-start(f32[128]{0:T(128)} %get-tuple-element.150) | copy-start | bytes 1540
  236.3 6.6 %copy-start.15 = (f32[128]{0:T(128)S(1)}, f32[128]{0:T(128)}, u32[]{:S(2)}) copy-start(f32[128]{0:T(128)} %get-tuple-element.151) | copy-start | bytes 1540
  236.3 6.6 %copy-start.16 = (f32[128]{0:T(128)S(1)}, f32[128]{0:T(128)}, u32[]{:S(2)}) copy-start(f32[128]{0:T(128)} %get-tuple-element.152) | copy-start | bytes 1540
  236.3 6.6 %copy-start.17 = (f32[128]{0:T(128)S(1)}, f32[128]{0:T(128)}, u32[]{:S(2)}) copy-start(f32[128]{0:T(128)} %get-tuple-element.153) | copy-start | bytes 1540
  236.3 6.6 %copy-start.18 = (f32[128]{0:T(128)S(1)}, f32[128]{0:T(128)}, u32[]{:S(2)}) copy-start(f32[128]{0:T(128)} %get-tuple-element.154) | copy-start | bytes 1540
  236.3 6.6 %copy-start.19 = (f32[128]{0:T(128)S(1)}, f32[128]{0:T(128)}, u32[]{:S(2)}) copy-start(f32[128]{0:T(128)} %get-tuple-element.155) | copy-start | bytes 1540
  236.3 6.6 %copy-start.20 = (f32[128]{0:T(128)S(1)}, f32[128]{0:T(128)}, u32[]{:S(2)}) copy-start(f32[128]{0:T(128)} %get-tuple-element.156) | copy-start | bytes 1540
  236.4 6.6 %copy-start.21 = (f32[128]{0:T(128)S(1)}, f32[128]{0:T(128)}, u32[]{:S(2)}) copy-start(f32[128]{0:T(128)} %get-tuple-element.126) | copy-start | bytes 1540
  236.4 6.6 %copy-start.22 = (f32[128]{0:T(128)S(1)}, f32[128]{0:T(128)}, u32[]{:S(2)}) copy-start(f32[128]{0:T(128)} %get-tuple-element.127) | copy-start | bytes 1540
  236.4 6.6 %copy-start.23 = (f32[128]{0:T(128)S(1)}, f32[128]{0:T(128)}, u32[]{:S(2)}) copy-start(f32[128]{0:T(128)} %get-tuple-element.128) | copy-start | bytes 1540
  236.4 6.6 %copy-start.24 = (f32[128]{0:T(128)S(1)}, f32[128]{0:T(128)}, u32[]{:S(2)}) copy-start(f32[128]{0:T(128)} %get-tuple-element.129) | copy-start | bytes 1540
  236.4 6.6 %copy-start.25 = (f32[128]{0:T(128)S(1)}, f32[128]{0:T(128)}, u32[]{:S(2)}) copy-start(f32[128]{0:T(128)} %get-tuple-element.130) | copy-start | bytes 1540
  236.4 6.6 %copy-start.26 = (f32[128]{0:T(128)S(1)}, f32[128]{0:T(128)}, u32[]{:S(2)}) copy-start(f32[128]{0:T(128)} %get-tuple-element.131) | copy-start | bytes 1540
  236.4 6.6 %copy-start.27 = (f32[128]{0:T(128)S(1)}, f32[128]{0:T(128)}, u32[]{:S(2)}) copy-start(f32[128]{0:T(128)} %get-tuple-element.132) | copy-start | bytes 1540
  236.4 6.6 %copy-start.28 = (f32[128]{0:T(128)S(1)}, f32[128]{0:T(128)}, u32[]{:S(2)}) copy-start(f32[128]{0:T(128)} %get-tuple-element.133) | copy-start | bytes 1540
  236.4 6.6 %copy-start.29 = (f32[128]{0:T(128)S(1)}, f32[128]{0:T(128)}, u32[]{:S(2)}) copy-start(f32[128]{0:T(128)} %get-tuple-element.134) | copy-start | bytes 1540
  236.4 6.6 %copy-start.30 = (f32[128]{0:T(128)S(1)}, f32[128]{0:T(128)}, u32[]{:S(2)}) copy-start(f32[128]{0:T(128)} %get-tuple-element.135) | copy-start | bytes 1540
  236.5 6.6 %copy-start.31 = (f32[128]{0:T(128)S(1)}, f32[128]{0:T(128)}, u32[]{:S(2)}) copy-start(f32[128]{0:T(128)} %get-tuple-element.136) | copy-start | bytes 1540
  236.5 6.6 %copy-start.32 = (f32[128]{0:T(128)S(1)}, f32[128]{0:T(128)}, u32[]{:S(2)}) copy-start(f32[128]{0:T(128)} %get-tuple-element.137) | copy-start | bytes 1540
  236.5 6.6 %copy-start.33 = (f32[128]{0:T(128)S(1)}, f32[128]{0:T(128)}, u32[]{:S(2)}) copy-start(f32[128]{0:T(128)} %get-tuple-element.138) | copy-start | bytes 1540
  236.5 6.6 %copy-start.34 = (f32[128]{0:T(128)S(1)}, f32[128]{0:T(128)}, u32[]{:S(2)}) copy-start(f32[128]{0:T(128)} %get-tuple-element.139) | copy-start | bytes 1540
  236.5 6.6 %copy-start.35 = (f32[128]{0:T(128)S(1)}, f32[128]{0:T(128)}, u32[]{:S(2)}) copy-start(f32[128]{0:T(128)} %get-tuple-element.140) | copy-start | bytes 1540
  236.5 6.6 %copy-start.36 = (f32[128]{0:T(128)S(1)}, f32[128]{0:T(128)}, u32[]{:S(2)}) copy-start(f32[128]{0:T(128)} %get-tuple-element.141) | copy-start | bytes 1540
  236.5 6.6 %copy-start.37 = (f32[128]{0:T(128)S(1)}, f32[128]{0:T(128)}, u32[]{:S(2)}) copy-start(f32[128]{0:T(128)} %get-tuple-element.142) | copy-start | bytes 1540
  236.5 6.6 %copy-start.38 = (f32[128]{0:T(128)S(1)}, f32[128]{0:T(128)}, u32[]{:S(2)}) copy-start(f32[128]{0:T(128)} %get-tuple-element.143) | copy-start | bytes 1540
  236.5 6.6 %copy-start.39 = (f32[128]{0:T(128)S(1)}, f32[128]{0:T(128)}, u32[]{:S(2)}) copy-start(f32[128]{0:T(128)} %get-tuple-element.144) | copy-start | bytes 1540
  238.6 4.3 %collective-permute-start = (bf16[30,128]{1,0:T(8,128)(2,1)S(1)}, bf16[30,128]{1,0:T(8,128)(2,1)S(1)}, u32[]{:S(2)}, u32[]{:S(2)}) collective-permute-start(bf16[30,128]{1,0:T(8,128)(2,1)S(1)} %slice.369), channel_id=1, source_target_pairs={{0,8},{8,16},{16,24},{24,32},{32,40},{40,48},{48,56},{56,64},{64,7... | collective-permute-start | bytes 23048 | tf_op jit(solution)/shard_map/ppermute | solution.py:76
  245.3 10.3 %all-to-all-start.1 = ((f32[8,1,768]{2,1,0:T(1,128)}), f32[8,1,768]{2,1,0:T(1,128)}, u32[]{:S(2)}, u32[]{:S(2)}) async-start(f32[8,1,768]{2,1,0:T(1,128)} %broadcast_in_dim.89), calls=%async_computation.1 | async-start | bytes 49152 | tf_op jit(solution)/shard_map/all_to_all | solution.py:24
  257.3 17.8 %all-to-all-start = ((bf16[16,129,128]{2,1,0:T(8,128)(2,1)}), bf16[16,129,128]{2,1,0:T(8,128)(2,1)}, u32[]{:S(2)}, u32[]{:S(2)}) async-start(bf16[16,129,128]{2,1,0:T(8,128)(2,1)} %broadcast_in_dim.85), calls=%async_computation | async-start | bytes 1114112 | tf_op jit(solution)/shard_map/all_to_all | solution.py:24
  266.6 11.1 %copy-start.5 = (f32[128,6,128]{0,2,1:T(8,128)S(1)}, f32[128,6,128]{0,2,1:T(8,128)}, u32[]{:S(2)}) copy-start(f32[128,6,128]{0,2,1:T(8,128)} %copy-done.4) | copy-start | bytes 1179652
  266.6 11.5 %copy-start.41 = (f32[128]{0:T(128)S(1)}, f32[128]{0:T(128)}, u32[]{:S(2)}) copy-start(f32[128]{0:T(128)} %param.34) | copy-start | bytes 1540
  275.1 2.6 copy-start.6
  275.1 2.6 copy-start.10
  275.1 2.7 copy-start.11
  278.2 2.1 copy-start.8
  320.0 3.4 %copy-start.2 = (bf16[768,2048]{1,0:T(8,128)(2,1)S(1)}, bf16[768,2048]{1,0:T(8,128)(2,1)}, u32[]{:S(2)}) copy-start(bf16[768,2048]{1,0:T(8,128)(2,1)} %copy-done.1) | copy-start | bytes 9437188
  320.0 3.5 %copy-start.7 = (bf16[96,2,8,256]{3,0,2,1:T(8,128)(2,1)S(1)}, bf16[96,2,8,256]{3,0,2,1:T(8,128)(2,1)}, u32[]{:S(2)}) copy-start(bf16[96,2,8,256]{3,0,2,1:T(8,128)(2,1)} %copy.79) | copy-start | bytes 2359300
Sparse Core Ops, SparseCore 0:
  9.4 44.8 all-gather.8
  56.0 28.8 all-gather.4
  87.1 55.7 all-gather.6
  144.4 49.7 all-gather.10
where the time goes:
time: 338 us; the launch traced here: 333 us
  waiting for transfers between devices  130 us (38%)
  matrix products  58.7 us (17%)
  other arithmetic  47.2 us (14%)
  local copies, waits for them, and re-layouts  36.5 us (11%)
  blocking collectives  30.8 us (9%)
  starting transfers between devices  15.8 us (5%)
  between operations  13.9 us (4%)
    all_gather x3, waiting for transfers between devices, in_one_piece(): lax.all_gather(both, axis, axis=dim, tiled=True)  88.9 us
    all_gather x1, waiting for transfers between devices, local(): lax.all_gather(tokens, 'tp', axis=0, tiled=True)  28.2 us
    dot_general x12, other arithmetic, block_step(): scores = jnp.einsum('htd,hsd,htsd->hts', query, input_gate, weight)  20.5 us
    dot_general x8, matrix products, local(): jnp.dot(normed, portion, preferred_element_type=jnp.float32)  20.5 us
    all_to_all x1, blocking collectives, local(): lax.all_to_all(projected[0], 'tp', split_axis=2, concat_axis=0, tiled=True)  18.2 us
    dot_general x12, matrix products, block_step(): jnp.einsum('htd,hdv->htv', query * jnp.exp(cumulative), state)  18.2 us
    all_to_all x2, starting transfers between devices, sent_to_all(): lax.all_to_all(jnp.broadcast_to(array[None], (size, *array.shape)), axis,...  12.6 us
    all_to_all x1, blocking collectives, local(): lax.all_to_all(both, 'tp', split_axis=0, concat_axis=2, tiled=True)  12.6 us
  transfers between devices with their start and end apart: 7, of which 5 were waited for; matrix products, arithmetic and copies ran while one was open for 37% of the time, Pallas kernels for 0%

commit v1 on v0

--- a/solution.py
+++ b/solution.py
@@ -8,6 +8,32 @@
 KW = 31
 BLOCK = 64
 EPSILON = 1e-06
+
+
+def post_figure(point):
+    which_axis = "tp"
+    block_last, x_new, fresh = (
+        lax.axis_size(which_axis),
+        lax.axis_index(which_axis),
+        point.shape[0],
+    )
+    history = list(map(lambda rr: (rr, (rr + 1) % block_last), range(block_last)))
+    entries = list(map(lambda rr: (rr, (rr - 1) % block_last), range(block_last)))
+    local_part = jnp.zeros((*point.shape[:0], block_last * fresh, *point.shape[1:]), point.dtype)
+    odd = met_up = point
+    u_next = block_last // 2
+    local_part = lax.dynamic_update_slice_in_dim(local_part, point, x_new * fresh, axis=0)
+    for s in range(1, u_next + 1):
+        odd = lax.ppermute(odd, axis_name=which_axis, perm=history)
+        local_part = lax.dynamic_update_slice_in_dim(
+            local_part, odd, (x_new - s) % block_last * fresh, axis=0
+        )
+        if s < block_last - u_next:
+            met_up = lax.ppermute(met_up, axis_name=which_axis, perm=entries)
+            local_part = lax.dynamic_update_slice_in_dim(
+                local_part, met_up, (x_new + s) % block_last * fresh, axis=0
+            )
+    return local_part
 
 
 def in_one_piece(arrays, axis, dim, along):
@@ -129,7 +155,7 @@
     w_out_conv,
 ):
     tp_count = lax.axis_size("tp")
-    normed = normalize_rows(lax.all_gather(tokens, "tp", axis=0, tiled=True), norm_gain)
+    normed = normalize_rows(post_figure(tokens), norm_gain)
     row_count = normed.shape[0]
     weights = (
         w_query,

time: 338 us -> 307 us (0.908)
  waiting for transfers between devices: 130 us -> 91 us
  starting transfers between devices: 15.8 us -> 26.5 us
    all_gather x1 -> x0, waiting for transfers between devices: 28.2 us -> none  [local(): lax.all_gather(tokens, 'tp', axis=0, tiled=True)]
    all_gather x3, waiting for transfers between devices: 88.9 us -> 65.3 us  [in_one_piece(): lax.all_gather(both, axis, axis=dim, tiled=True)]
    ppermute x0 -> x7, waiting for transfers between devices: none -> 13.8 us  [the longest x4 12.8 us: post_figure(): odd = lax.ppermute(odd, axis_name=which_axis, perm=history)]
    ppermute x0 -> x7, starting transfers between devices: none -> 10.8 us  [the longest x4 9.93 us: post_figure(): odd = lax.ppermute(odd, axis_name=which_axis, perm=history)]
    unnamed x92 -> x90, local copies, waits for them, and re-layouts: 7.34 us -> 7.22 us
  transfers between devices with their start and end apart: 7 -> 13, of which waited for: 5 -> 10; matrix products, arithmetic and copies ran while one was open for 37% -> 41% of each run, Pallas kernels for 0% -> 0%
where the time goes in v1:
time: 307 us; the launch traced here: 302 us
  waiting for transfers between devices  91 us (30%)
  matrix products  58.6 us (19%)
  other arithmetic  45.2 us (15%)
  local copies, waits for them, and re-layouts  35.9 us (12%)
  blocking collectives  30.8 us (10%)
  starting transfers between devices  26.5 us (9%)
  between operations  14 us (5%)
    all_gather x3, waiting for transfers between devices, in_one_piece(): lax.all_gather(both, axis, axis=dim, tiled=True)  65.3 us
    dot_general x12, other arithmetic, block_step(): scores = jnp.einsum('htd,hsd,htsd->hts', query, input_gate, weight)  20.5 us
    dot_general x8, matrix products, local(): jnp.dot(normed, portion, preferred_element_type=jnp.float32)  20.4 us
    all_to_all x1, blocking collectives, local(): lax.all_to_all(projected[0], 'tp', split_axis=2, concat_axis=0, tiled=True)  18.2 us
    dot_general x12, matrix products, block_step(): jnp.einsum('htd,hdv->htv', query * jnp.exp(cumulative), state)  18.2 us
    ppermute x4, waiting for transfers between devices, post_figure(): odd = lax.ppermute(odd, axis_name=which_axis, perm=history)  12.8 us
    all_to_all x1, blocking collectives, local(): lax.all_to_all(both, 'tp', split_axis=0, concat_axis=2, tiled=True)  12.5 us
    all_to_all x2, starting transfers between devices, sent_to_all(): lax.all_to_all(jnp.broadcast_to(array[None], (size, *array.shape)), axis,...  12.4 us
  transfers between devices with their start and end apart: 13, of which 10 were waited for; matrix products, arithmetic and copies ran while one was open for 41% of the time, Pallas kernels for 0%

profile of v1, /device:TPU:1, one launch (start us, length us, event | category | flops | bytes accessed | tf_op | source)
XLA Modules:
  0.0 302.4 jit_solution(7100822343950329148)
XLA Ops:
  6.5 1.4 pad_maximum_fusion.3
  15.2 2.6 collective-permute-start
  17.8 1.6 slice_bitcast_fusion.35
  19.3 1.6 slice_bitcast_fusion.36
  22.8 2.4 collective-permute-start.2
  25.3 4.6 %collective-permute-done.2 = bf16[96,2048]{1,0:T(8,128)(2,1)S(1)} collective-permute-done((bf16[96,2048]{1,0:T(8,128)(2,1)S(1)}, bf16[96,2048]{1,0:T(8,128)(2,1)S(1)}, u32[]{:S(2)}, u32[]{:S(2)}) %collective-permute-start.2) | collective-permute-done | bytes 393248 | tf_op jit(solution)/shard_map/ppermute | solution.py:27
  29.9 2.5 collective-permute-start.4
  33.7 3.4 %collective-permute-done.4 = bf16[96,2048]{1,0:T(8,128)(2,1)S(1)} collective-permute-done((bf16[96,2048]{1,0:T(8,128)(2,1)S(1)}, bf16[96,2048]{1,0:T(8,128)(2,1)S(1)}, u32[]{:S(2)}, u32[]{:S(2)}) %collective-permute-start.4) | collective-permute-done | bytes 393248 | tf_op jit(solution)/shard_map/ppermute | solution.py:27
  37.1 2.5 collective-permute-start.6
  40.3 4.0 %collective-permute-done.6 = bf16[96,2048]{1,0:T(8,128)(2,1)S(1)} collective-permute-done((bf16[96,2048]{1,0:T(8,128)(2,1)S(1)}, bf16[96,2048]{1,0:T(8,128)(2,1)S(1)}, u32[]{:S(2)}, u32[]{:S(2)}) %collective-permute-start.6) | collective-permute-done | bytes 393248 | tf_op jit(solution)/shard_map/ppermute | solution.py:27
  45.9 8.5 %all-gather.6.cloned.1.call-done = bf16[256,2048]{1,0:T(8,128)(2,1)} async-done(((bf16[256,128]{1,0:T(8,128)(2,1)}), bf16[256,2048]{1,0:T(8,128)(2,1)}) %all-gather.6.cloned.1.call-update) | async-done | bytes 1048592 | tf_op jit(solution)/shard_map/all_gather | solution.py:45
  54.4 1.3 fusion.138
  55.7 1.1 pad_maximum_fusion
  56.8 56.8 %all-gather.4.cloned.1.call-done = bf16[2048,1280]{1,0:T(8,128)(2,1)} async-done(((bf16[128,1280]{1,0:T(8,128)(2,1)}), bf16[2048,1280]{1,0:T(8,128)(2,1)}) %all-gather.4.cloned.1.call-update) | async-done | bytes 5242896 | tf_op jit(solution)/shard_map/all_gather | solution.py:45
  113.5 2.8 divide_multiply_fusion
  116.3 2.1 convolution_convert_fusion.6
  118.4 2.9 log-plus-one_add_fusion
  121.4 80.2 %while.13 = (s32[]{:T(128)}, f32[1,128,128]{2,1,0:T(8,128)S(1)}, f32[12,1,64,128]{3,2,1,0:T(8,128)}, f32[12,1,64,128]{3,2,1,0:T(8,128)}, f32[12,1,64,128]{3,2,1,...) while((s32[]{:T(128)}, f32[1,128,128]{2,1,0:T(8,128)S(1)}, ...), condition=%wide.region_3.4_spmd.clone, body=%wide.region_1.3_spmd.clone.sunk | while | flops 9003011 | bytes 5051520 | solution.py:209
  123.6 1.7 fusion.167
  125.5 1.5 fusion.169
  127.1 1.0 fusion.166
  130.3 1.7 fusion.167
  132.2 1.5 fusion.169
  137.0 1.7 fusion.167
  138.9 1.5 fusion.169
  143.7 1.7 fusion.167
  145.6 1.5 fusion.169
  150.4 1.7 fusion.167
  152.3 1.5 fusion.169
  157.1 1.7 fusion.167
  158.9 1.5 fusion.169
  163.7 1.7 fusion.167
  165.6 1.5 fusion.169
  170.4 1.7 fusion.167
  172.3 1.5 fusion.169
  177.1 1.7 fusion.167
  179.0 1.5 fusion.169
  183.8 1.7 fusion.167
  185.7 1.5 fusion.169
  190.4 1.7 fusion.167
  192.3 1.5 fusion.169
  197.1 1.7 fusion.167
  199.0 1.5 fusion.169
  201.5 1.2 fusion.85
  203.6 1.1 broadcast_add_fusion
  204.8 2.2 fusion.66
  207.2 2.0 fusion.69
  209.2 3.3 %collective-permute-start.7 = (bf16[30,128]{1,0:T(8,128)(2,1)S(1)}, bf16[30,128]{1,0:T(8,128)(2,1)S(1)}, u32[]{:S(2)}, u32[]{:S(2)}) collective-permute-start(bf16[30,128]{1,0:T(8,128)(2,1)S(1)} %slice.369), channel_id=1, source_target_pairs={{0,8},{8,16},{16,24},{24,32},{32,40},{40,48},{48,56},{56,64},{64,7... | collective-permute-start | bytes 23048 | tf_op jit(solution)/shard_map/ppermute | solution.py:102
  214.0 1.5 multiply_reduce_fusion
  216.2 5.4 %all-to-all-start.1 = ((f32[8,1,768]{2,1,0:T(1,128)}), f32[8,1,768]{2,1,0:T(1,128)}, u32[]{:S(2)}, u32[]{:S(2)}) async-start(f32[8,1,768]{2,1,0:T(1,128)} %broadcast_in_dim.93), calls=%async_computation.1 | async-start | bytes 49152 | tf_op jit(solution)/shard_map/all_to_all | solution.py:50
  221.5 1.4 pad_maximum_fusion.4
  222.9 3.4 %all-to-all-done.1 = f32[8,1,768]{2,1,0:T(1,128)} async-done(((f32[8,1,768]{2,1,0:T(1,128)}), f32[8,1,768]{2,1,0:T(1,128)}, u32[]{:S(2)}, u32[]{:S(2)}) %all-to-all-start.1) | async-done | bytes 24608 | tf_op jit(solution)/shard_map/all_to_all | solution.py:50
  226.3 1.7 broadcast_in_dim.89
  228.0 7.0 %all-to-all-start = ((bf16[16,129,128]{2,1,0:T(8,128)(2,1)}), bf16[16,129,128]{2,1,0:T(8,128)(2,1)}, u32[]{:S(2)}, u32[]{:S(2)}) async-start(bf16[16,129,128]{2,1,0:T(8,128)(2,1)} %broadcast_in_dim.89), calls=%async_computation | async-start | bytes 1114112 | tf_op jit(solution)/shard_map/all_to_all | solution.py:50
  235.8 1.5 multiply_convert_fusion
  237.3 8.4 %all-to-all-done = bf16[16,129,128]{2,1,0:T(8,128)(2,1)} async-done(((bf16[16,129,128]{2,1,0:T(8,128)(2,1)}), bf16[16,129,128]{2,1,0:T(8,128)(2,1)}, u32[]{:S(2)}, u32[]{:S(2)}) %all-to-all-start) | async-done | bytes 528416 | tf_op jit(solution)/shard_map/all_to_all | solution.py:50
  246.8 1.2 select_bitcast_fusion
  248.9 2.1 fusion.117
  251.0 12.5 %all_to_all.44 = bf16[8,96,256]{2,1,0:T(8,128)(2,1)S(1)} all-to-all(bf16[8,96,256]{2,1,0:T(8,128)(2,1)S(1)} %bitcast.263), channel_id=1, replica_groups=mesh['sp'=16,'tp'=8] {'tp'}, dimensions={0} | all-to-all | bytes 786432 | tf_op jit(solution)/shard_map/all_to_all | solution.py:248
  263.7 3.0 fusion.44
  266.7 3.0 fusion.41
  270.5 18.2 %all_to_all.45 = bf16[96,2,2048]{0,1,2:T(2,128)(2,1)S(1)} all-to-all(bf16[96,2,2048]{0,1,2:T(2,128)(2,1)S(1)} %copy.78), channel_id=1, replica_groups=mesh['sp'=16,'tp'=8] {'tp'}, dimensions={2} | all-to-all | bytes 1572864 | tf_op jit(solution)/shard_map/all_to_all | solution.py:256
  289.5 3.3 %fusion.60 = f32[768,256]{1,0:T(8,128)S(1)} fusion(bf16[768,2048]{1,0:T(8,128)(2,1)} %copy-done, bf16[2048,1280]{1,0:T(8,128)(2,1)} %all-gather.4.cloned.1.call-done, bf16[768,2,256]{2,0,1:T(8,128)(2,1)S(1)} %bitcast.268), kind=kOutput, calls=%fused_computation.65 | convolution fusion | flops 806682624 | bytes 5373952 | tf_op jit(solution)/shard_map/dot_general | solution.py:186
  292.9 3.0 fusion.54
  (253 shorter events, 59.9 us)
Async XLA Ops:
  6.5 15.5 %copy-start.8 = (bf16[96,2048]{1,0:T(8,128)(2,1)S(1)}, bf16[96,2048]{1,0:T(8,128)(2,1)}, u32[]{:S(2)}) copy-start(bf16[96,2048]{1,0:T(8,128)(2,1)} %param.21) | copy-start | bytes 1179652
  6.5 47.8 %all-gather.6.cloned.1.call-start = ((), (), s32[]{:S(2)}) async-start(), calls=%async_computation.5 | async-start | bytes 1114112 | tf_op jit(solution)/shard_map/all_gather | solution.py:45
  8.0 105.5 %all-gather.4.cloned.1.call-start = ((), (), s32[]{:S(2)}) async-start(), calls=%async_computation.4 | async-start | bytes 5570560 | tf_op jit(solution)/shard_map/all_gather | solution.py:45
  14.4 0.7 copy-start.7
  15.1 248.6 %all-gather.8.cloned.1.call-start = ((), (), s32[]{:S(2)}) async-start(), calls=%async_computation.6 | async-start | bytes 9437184 | tf_op jit(solution)/shard_map/all_gather | solution.py:45
  15.2 7.6 %collective-permute-start = (bf16[96,2048]{1,0:T(8,128)(2,1)}, bf16[96,2048]{1,0:T(8,128)(2,1)S(1)}, u32[]{:S(2)}, u32[]{:S(2)}) collective-permute-start(bf16[96,2048]{1,0:T(8,128)(2,1)} %param.21), channel_id=1, source_target_pairs={{0,1},{1,2},{2,3},{3,4},{4,5},{5,6},{6,7},{7,0},{8,9},{9,10},{10,1... | collective-permute-start | bytes 1179656 | tf_op jit(solution)/shard_map/ppermute | solution.py:27
  17.8 7.4 %collective-permute-start.1 = (bf16[96,2048]{1,0:T(8,128)(2,1)}, bf16[96,2048]{1,0:T(8,128)(2,1)S(1)}, u32[]{:S(2)}, u32[]{:S(2)}) collective-permute-start(bf16[96,2048]{1,0:T(8,128)(2,1)} %param.21), channel_id=1, source_target_pairs={{0,7},{1,0},{2,1},{3,2},{4,3},{5,4},{6,5},{7,6},{8,15},{9,8},{10,9... | collective-permute-start | bytes 1179656 | tf_op jit(solution)/shard_map/ppermute | solution.py:32
  22.8 7.1 %collective-permute-start.2 = (bf16[96,2048]{1,0:T(8,128)(2,1)S(1)}, bf16[96,2048]{1,0:T(8,128)(2,1)S(1)}, u32[]{:S(2)}, u32[]{:S(2)}) collective-permute-start(bf16[96,2048]{1,0:T(8,128)(2,1)S(1)} %collective-permute-done), channel_id=1, source_target_pairs={{0,1},{1,2},{2,3},{3,4},{4,5},{5,6},{6,7},{7,0},{8,9},{9,10},{10,1... | collective-permute-start | bytes 1179656 | tf_op jit(solution)/shard_map/ppermute | solution.py:27
  25.2 7.6 %collective-permute-start.3 = (bf16[96,2048]{1,0:T(8,128)(2,1)S(1)}, bf16[96,2048]{1,0:T(8,128)(2,1)S(1)}, u32[]{:S(2)}, u32[]{:S(2)}) collective-permute-start(bf16[96,2048]{1,0:T(8,128)(2,1)S(1)} %collective-permute-done.1), channel_id=1, source_target_pairs={{0,7},{1,0},{2,1},{3,2},{4,3},{5,4},{6,5},{7,6},{8,15},{9,8},{10,9... | collective-permute-start | bytes 1179656 | tf_op jit(solution)/shard_map/ppermute | solution.py:32
  29.9 7.2 %collective-permute-start.4 = (bf16[96,2048]{1,0:T(8,128)(2,1)S(1)}, bf16[96,2048]{1,0:T(8,128)(2,1)S(1)}, u32[]{:S(2)}, u32[]{:S(2)}) collective-permute-start(bf16[96,2048]{1,0:T(8,128)(2,1)S(1)} %collective-permute-done.2), channel_id=1, source_target_pairs={{0,1},{1,2},{2,3},{3,4},{4,5},{5,6},{6,7},{7,0},{8,9},{9,10},{10,1... | collective-permute-start | bytes 1179656 | tf_op jit(solution)/shard_map/ppermute | solution.py:27
  32.8 7.5 %collective-permute-start.5 = (bf16[96,2048]{1,0:T(8,128)(2,1)S(1)}, bf16[96,2048]{1,0:T(8,128)(2,1)S(1)}, u32[]{:S(2)}, u32[]{:S(2)}) collective-permute-start(bf16[96,2048]{1,0:T(8,128)(2,1)S(1)} %collective-permute-done.3), channel_id=1, source_target_pairs={{0,7},{1,0},{2,1},{3,2},{4,3},{5,4},{6,5},{7,6},{8,15},{9,8},{10,9... | collective-permute-start | bytes 1179656 | tf_op jit(solution)/shard_map/ppermute | solution.py:32
  33.6 11.4 %copy-start.11 = (f32[2048]{0:T(1024)S(1)}, f32[2048]{0:T(1024)}, u32[]{:S(2)}) copy-start(f32[2048]{0:T(1024)} %param.22) | copy-start | bytes 24580
  37.1 7.2 %collective-permute-start.6 = (bf16[96,2048]{1,0:T(8,128)(2,1)S(1)}, bf16[96,2048]{1,0:T(8,128)(2,1)S(1)}, u32[]{:S(2)}, u32[]{:S(2)}) collective-permute-start(bf16[96,2048]{1,0:T(8,128)(2,1)S(1)} %collective-permute-done.4), channel_id=1, source_target_pairs={{0,1},{1,2},{2,3},{3,4},{4,5},{5,6},{6,7},{7,0},{8,9},{9,10},{10,1... | collective-permute-start | bytes 1179656 | tf_op jit(solution)/shard_map/ppermute | solution.py:27
  45.8 203.0 %copy-start = (bf16[768,2048]{1,0:T(8,128)(2,1)}, bf16[768,2048]{1,0:T(8,128)(2,1)S(1)}, u32[]{:S(2)}) copy-start(bf16[768,2048]{1,0:T(8,128)(2,1)S(1)} %fusion.30) | copy-start | bytes 9437188
  116.3 2.1 copy-start.39
  202.8 0.8 copy-start.2
  204.8 8.4 %copy-start.3 = (f32[128,6,128]{0,2,1:T(8,128)}, f32[128,6,128]{0,2,1:T(8,128)S(1)}, u32[]{:S(2)}) copy-start(f32[128,6,128]{0,2,1:T(8,128)S(1)} %copy.72) | copy-start | bytes 1179652
  206.9 6.8 %copy-start.12 = (f32[128]{0:T(128)S(1)}, f32[128]{0:T(128)}, u32[]{:S(2)}) copy-start(f32[128]{0:T(128)} %get-tuple-element.149) | copy-start | bytes 1540
  207.0 6.8 %copy-start.13 = (f32[128]{0:T(128)S(1)}, f32[128]{0:T(128)}, u32[]{:S(2)}) copy-start(f32[128]{0:T(128)} %get-tuple-element.150) | copy-start | bytes 1540
  207.0 6.8 %copy-start.14 = (f32[128]{0:T(128)S(1)}, f32[128]{0:T(128)}, u32[]{:S(2)}) copy-start(f32[128]{0:T(128)} %get-tuple-element.151) | copy-start | bytes 1540
  207.0 6.8 %copy-start.15 = (f32[128]{0:T(128)S(1)}, f32[128]{0:T(128)}, u32[]{:S(2)}) copy-start(f32[128]{0:T(128)} %get-tuple-element.152) | copy-start | bytes 1540
  207.0 6.8 %copy-start.16 = (f32[128]{0:T(128)S(1)}, f32[128]{0:T(128)}, u32[]{:S(2)}) copy-start(f32[128]{0:T(128)} %get-tuple-element.153) | copy-start | bytes 1540
  207.0 6.8 %copy-start.17 = (f32[128]{0:T(128)S(1)}, f32[128]{0:T(128)}, u32[]{:S(2)}) copy-start(f32[128]{0:T(128)} %get-tuple-element.154) | copy-start | bytes 1540
  207.0 6.8 %copy-start.18 = (f32[128]{0:T(128)S(1)}, f32[128]{0:T(128)}, u32[]{:S(2)}) copy-start(f32[128]{0:T(128)} %get-tuple-element.155) | copy-start | bytes 1540
  207.0 6.8 %copy-start.19 = (f32[128]{0:T(128)S(1)}, f32[128]{0:T(128)}, u32[]{:S(2)}) copy-start(f32[128]{0:T(128)} %get-tuple-element.156) | copy-start | bytes 1540
  207.0 6.8 %copy-start.20 = (f32[128]{0:T(128)S(1)}, f32[128]{0:T(128)}, u32[]{:S(2)}) copy-start(f32[128]{0:T(128)} %get-tuple-element.126) | copy-start | bytes 1540
  207.0 6.8 %copy-start.21 = (f32[128]{0:T(128)S(1)}, f32[128]{0:T(128)}, u32[]{:S(2)}) copy-start(f32[128]{0:T(128)} %get-tuple-element.127) | copy-start | bytes 1540
  207.0 6.8 %copy-start.22 = (f32[128]{0:T(128)S(1)}, f32[128]{0:T(128)}, u32[]{:S(2)}) copy-start(f32[128]{0:T(128)} %get-tuple-element.128) | copy-start | bytes 1540
  207.1 6.8 %copy-start.23 = (f32[128]{0:T(128)S(1)}, f32[128]{0:T(128)}, u32[]{:S(2)}) copy-start(f32[128]{0:T(128)} %get-tuple-element.129) | copy-start | bytes 1540
  207.1 6.8 %copy-start.24 = (f32[128]{0:T(128)S(1)}, f32[128]{0:T(128)}, u32[]{:S(2)}) copy-start(f32[128]{0:T(128)} %get-tuple-element.130) | copy-start | bytes 1540
  207.1 6.8 %copy-start.25 = (f32[128]{0:T(128)S(1)}, f32[128]{0:T(128)}, u32[]{:S(2)}) copy-start(f32[128]{0:T(128)} %get-tuple-element.131) | copy-start | bytes 1540
  207.1 6.8 %copy-start.26 = (f32[128]{0:T(128)S(1)}, f32[128]{0:T(128)}, u32[]{:S(2)}) copy-start(f32[128]{0:T(128)} %get-tuple-element.132) | copy-start | bytes 1540
  207.1 6.8 %copy-start.27 = (f32[128]{0:T(128)S(1)}, f32[128]{0:T(128)}, u32[]{:S(2)}) copy-start(f32[128]{0:T(128)} %get-tuple-element.133) | copy-start | bytes 1540
  207.1 6.8 %copy-start.28 = (f32[128]{0:T(128)S(1)}, f32[128]{0:T(128)}, u32[]{:S(2)}) copy-start(f32[128]{0:T(128)} %get-tuple-element.134) | copy-start | bytes 1540
  207.1 6.8 %copy-start.29 = (f32[128]{0:T(128)S(1)}, f32[128]{0:T(128)}, u32[]{:S(2)}) copy-start(f32[128]{0:T(128)} %get-tuple-element.135) | copy-start | bytes 1540
  207.1 6.8 %copy-start.30 = (f32[128]{0:T(128)S(1)}, f32[128]{0:T(128)}, u32[]{:S(2)}) copy-start(f32[128]{0:T(128)} %get-tuple-element.136) | copy-start | bytes 1540
  207.1 6.8 %copy-start.31 = (f32[128]{0:T(128)S(1)}, f32[128]{0:T(128)}, u32[]{:S(2)}) copy-start(f32[128]{0:T(128)} %get-tuple-element.137) | copy-start | bytes 1540
  207.1 6.8 %copy-start.32 = (f32[128]{0:T(128)S(1)}, f32[128]{0:T(128)}, u32[]{:S(2)}) copy-start(f32[128]{0:T(128)} %get-tuple-element.138) | copy-start | bytes 1540
  207.2 6.8 %copy-start.33 = (f32[128]{0:T(128)S(1)}, f32[128]{0:T(128)}, u32[]{:S(2)}) copy-start(f32[128]{0:T(128)} %get-tuple-element.139) | copy-start | bytes 1540
  207.2 6.8 %copy-start.34 = (f32[128]{0:T(128)S(1)}, f32[128]{0:T(128)}, u32[]{:S(2)}) copy-start(f32[128]{0:T(128)} %get-tuple-element.140) | copy-start | bytes 1540
  207.2 6.8 %copy-start.35 = (f32[128]{0:T(128)S(1)}, f32[128]{0:T(128)}, u32[]{:S(2)}) copy-start(f32[128]{0:T(128)} %get-tuple-element.141) | copy-start | bytes 1540
  207.2 6.8 %copy-start.36 = (f32[128]{0:T(128)S(1)}, f32[128]{0:T(128)}, u32[]{:S(2)}) copy-start(f32[128]{0:T(128)} %get-tuple-element.142) | copy-start | bytes 1540
  207.2 6.8 %copy-start.37 = (f32[128]{0:T(128)S(1)}, f32[128]{0:T(128)}, u32[]{:S(2)}) copy-start(f32[128]{0:T(128)} %get-tuple-element.143) | copy-start | bytes 1540
  207.2 6.8 %copy-start.38 = (f32[128]{0:T(128)S(1)}, f32[128]{0:T(128)}, u32[]{:S(2)}) copy-start(f32[128]{0:T(128)} %get-tuple-element.144) | copy-start | bytes 1540
  209.2 4.5 %collective-permute-start.7 = (bf16[30,128]{1,0:T(8,128)(2,1)S(1)}, bf16[30,128]{1,0:T(8,128)(2,1)S(1)}, u32[]{:S(2)}, u32[]{:S(2)}) collective-permute-start(bf16[30,128]{1,0:T(8,128)(2,1)S(1)} %slice.369), channel_id=1, source_target_pairs={{0,8},{8,16},{16,24},{24,32},{32,40},{40,48},{48,56},{56,64},{64,7... | collective-permute-start | bytes 23048 | tf_op jit(solution)/shard_map/ppermute | solution.py:102
  216.2 10.2 %all-to-all-start.1 = ((f32[8,1,768]{2,1,0:T(1,128)}), f32[8,1,768]{2,1,0:T(1,128)}, u32[]{:S(2)}, u32[]{:S(2)}) async-start(f32[8,1,768]{2,1,0:T(1,128)} %broadcast_in_dim.93), calls=%async_computation.1 | async-start | bytes 49152 | tf_op jit(solution)/shard_map/all_to_all | solution.py:50
  228.0 17.8 %all-to-all-start = ((bf16[16,129,128]{2,1,0:T(8,128)(2,1)}), bf16[16,129,128]{2,1,0:T(8,128)(2,1)}, u32[]{:S(2)}, u32[]{:S(2)}) async-start(bf16[16,129,128]{2,1,0:T(8,128)(2,1)} %broadcast_in_dim.89), calls=%async_computation | async-start | bytes 1114112 | tf_op jit(solution)/shard_map/all_to_all | solution.py:50
  237.3 11.1 %copy-start.4 = (f32[128,6,128]{0,2,1:T(8,128)S(1)}, f32[128,6,128]{0,2,1:T(8,128)}, u32[]{:S(2)}) copy-start(f32[128,6,128]{0,2,1:T(8,128)} %copy-done.3) | copy-start | bytes 1179652
  237.3 11.6 %copy-start.40 = (f32[128]{0:T(128)S(1)}, f32[128]{0:T(128)}, u32[]{:S(2)}) copy-start(f32[128]{0:T(128)} %param.34) | copy-start | bytes 1540
  245.8 2.6 copy-start.5
  245.8 2.6 copy-start.9
  245.8 2.7 copy-start.10
  248.9 2.1 copy-start.6
  289.5 3.3 %copy-start.1 = (bf16[768,2048]{1,0:T(8,128)(2,1)S(1)}, bf16[768,2048]{1,0:T(8,128)(2,1)}, u32[]{:S(2)}) copy-start(bf16[768,2048]{1,0:T(8,128)(2,1)} %copy-done) | copy-start | bytes 9437188
Sparse Core Ops, SparseCore 0:
  9.4 44.8 all-gather.5
  56.5 57.0 all-gather.3
  115.3 49.7 all-gather.7
